TPU v7x, 256 devices: a whole 4x4x8 slice. The times are simulated.
256 devices in a mesh: kv: 16 (over y, x), tp: 16 (over z, core).
Axes of the slice: x: 4, y: 4, z: 8, core: 2. Of those that a mesh axis runs over, the one named last changes fastest.
Arguments:
- tokens: bfloat16 [128, 4096], P(None, ('kv', 'tp')), may hold values from -41 to 41
- lengths: int32 [128], P('kv'), may hold values from 1 to 8192, 262144 in all
- retention_state: float32 [128, 16, 128, 256], P('kv', 'tp'), may hold values from -4 to 4
- mixer_gain: float32 [4096], P('kv'), may hold values from 0.1 to 1.9
- query_weight: bfloat16 [4096, 2048], P('kv', 'tp'), may hold values from -0.09375 to 0.09375
- key_weight: bfloat16 [4096, 2048], P('kv', 'tp'), may hold values from -0.09375 to 0.09375
- value_weight: bfloat16 [4096, 4096], P('kv', 'tp'), may hold values from -0.09375 to 0.09375
- gate_weight: bfloat16 [4096, 4096], P('kv', 'tp'), may hold values from -0.09375 to 0.09375
- output_weight: bfloat16 [4096, 4096], P('tp', 'kv'), may hold values from -0.125 to 0.125
- channel_gain: float32 [4096], P('kv'), may hold values from 0.1 to 1.9
- ffn_gate: bfloat16 [4096, 11264], P('kv', 'tp'), may hold values from -0.09375 to 0.09375
- ffn_up: bfloat16 [4096, 11264], P('kv', 'tp'), may hold values from -0.09375 to 0.09375
- ffn_down: bfloat16 [11264, 4096], P('tp', 'kv'), may hold values from -0.078125 to 0.078125
Outputs:
- layer_output: bfloat16 [128, 4096], P(None, ('kv', 'tp'))
- new_state: float32 [128, 16, 128, 256], P('kv', 'tp')
All inputs are finite; a program needn't handle non-finite values. No bound on the sum of `lengths` on one device may be relied on, other than what follows from the above.
Results may differ from a plain program's by a relative error of at most 0.022.
Values may be sent and summed in bfloat16 or wider, within the bound.
No kernel may reach another device: no remote copies, remote signals or barrier semaphores. Data moves between devices by JAX's collectives and lax.ppermute only.
A program may use at most 64 MiB of HBM per device.

v0:
```python
import jax
import jax.numpy as jnp
from jax import lax
from jax.sharding import PartitionSpec as P

D = 4096
HEADS = 16
QK = 128


def in_blocks(value, dim, devices):
    lengths = value.shape
    blocks = value.reshape(*lengths[:dim], devices, lengths[dim] // devices, *lengths[dim + 1 :])
    return jnp.moveaxis(blocks, dim, 0)


def sent_and_summed(value, axis, dim):
    blocks = in_blocks(value, dim, lax.axis_size(axis))
    arrived = lax.all_to_all(blocks, axis, split_axis=0, concat_axis=0, tiled=True)
    return arrived.astype(jnp.float32).sum(axis=0)


def in_one_piece(arrays, axis, dim, along):
    columns = [a.reshape(*a.shape[:along], -1) for a in arrays]
    both = jnp.concatenate(columns, axis=along)
    result, at, finished = (sent_and_summed(both, axis, dim), 0, [])
    for a, column in zip(arrays, columns):
        piece = result[..., at : at + column.shape[along]]
        finished.append(piece.reshape(*piece.shape[:along], *a.shape[along:]))
        at += column.shape[along]
    return tuple(finished)


def copy_for_each(value, axis):
    devices = lax.axis_size(axis)
    return lax.all_to_all(
        jnp.broadcast_to(value[None], (devices, *value.shape)), axis, 0, 0, tiled=True
    )


def joined_along(blocks, dim):
    blocks = jnp.moveaxis(blocks, 0, dim)
    lengths = blocks.shape
    return blocks.reshape(*lengths[:dim], lengths[dim] * lengths[dim + 1], *lengths[dim + 2 :])


def gather_directly(value, axis, dim):
    blocks = copy_for_each(value, axis)
    return joined_along(blocks, dim)


def rotate_heads(vectors, positions):
    half_dim = vectors.shape[-1] // 2
    frequency = 10000.0 ** (-jnp.arange(half_dim, dtype=jnp.float32) / half_dim)
    angles = positions.astype(jnp.float32)[:, None, None] * frequency
    cosine = jnp.cos(angles)
    sine_part = jnp.sin(angles)
    first_half = vectors[..., :half_dim]
    second = vectors[..., half_dim:]
    return jnp.concatenate(
        [first_half * cosine - second * sine_part, first_half * sine_part + second * cosine],
        axis=-1,
    )


def gathered_rows(columns):
    return lax.all_gather(columns, "tp", axis=1, tiled=True)


def owned_sums(partial_value, squares):
    raw_sums, totals = in_one_piece(
        (partial_value.astype(jnp.bfloat16), squares.astype(jnp.bfloat16)), "kv", 0, 1
    )
    summed = raw_sums * lax.rsqrt(totals / D + 1e-06)[:, None]
    return summed


def on_device(
    tokens,
    lengths,
    retention_state,
    mixer_gain,
    query_weight,
    key_weight,
    value_weight,
    gate_weight,
    output_weight,
    channel_gain,
    ffn_gate,
    ffn_up,
    ffn_down,
):
    feature_block = gathered_rows(tokens).astype(jnp.float32)
    squares = jnp.sum(feature_block * feature_block, axis=1)
    normed = (feature_block * mixer_gain).astype(jnp.bfloat16)
    partial_value = jnp.concatenate(
        [
            jnp.dot(normed, query_weight, preferred_element_type=jnp.float32),
            jnp.dot(normed, key_weight, preferred_element_type=jnp.float32),
            jnp.dot(normed, value_weight, preferred_element_type=jnp.float32),
            jnp.dot(normed, gate_weight, preferred_element_type=jnp.float32),
        ],
        axis=1,
    )
    owned_rows = owned_sums(partial_value, squares)
    local_heads = query_weight.shape[1] // QK
    q_width = query_weight.shape[1]
    v_width = value_weight.shape[1]
    head_width = v_width // local_heads
    seq_rows = owned_rows.shape[0]
    query_rows = rotate_heads(
        owned_rows[:, :q_width].reshape(seq_rows, local_heads, QK), lengths
    ).astype(jnp.bfloat16)
    key_rows = (
        rotate_heads(
            owned_rows[:, q_width : 2 * q_width].reshape(seq_rows, local_heads, QK), lengths
        )
        * QK ** (-0.5)
    ).astype(jnp.bfloat16)
    value_rows = (
        owned_rows[:, 2 * q_width : 2 * q_width + v_width]
        .astype(jnp.bfloat16)
        .reshape(seq_rows, local_heads, head_width)
    )
    gate_rows = owned_rows[:, 2 * q_width + v_width :]
    head_ids = (lax.axis_index("tp") * local_heads + jnp.arange(local_heads)).astype(jnp.float32)
    decay_rate = 1.0 - 2.0 ** (-5.0 - 10.0 * head_ids / (HEADS - 1))
    new_state = (
        decay_rate[None, :, None, None] * retention_state
        + key_rows.astype(jnp.float32)[..., :, None] * value_rows.astype(jnp.float32)[..., None, :]
    )
    retained = jnp.einsum(
        "bhk,bhkv->bhv", query_rows.astype(jnp.float32), new_state, precision=lax.Precision.HIGHEST
    )
    normalized = retained * lax.rsqrt(jnp.mean(retained * retained, axis=-1) + 1e-06)[..., None]
    merged = (normalized.reshape(seq_rows, v_width) * jax.nn.silu(gate_rows)).astype(jnp.bfloat16)
    mixed_part = jnp.dot(
        gather_directly(merged, "kv", 0), output_weight, preferred_element_type=jnp.float32
    )
    mixed_cols = sent_and_summed(mixed_part.astype(jnp.bfloat16), "tp", 1)
    residual = (tokens.astype(jnp.float32) + mixed_cols).astype(jnp.bfloat16)
    block_two = gathered_rows(residual).astype(jnp.float32)
    squares_two = jnp.sum(block_two * block_two, axis=1)
    normed_two = (block_two * channel_gain).astype(jnp.bfloat16)
    partial_two = jnp.concatenate(
        [
            jnp.dot(normed_two, ffn_gate, preferred_element_type=jnp.float32),
            jnp.dot(normed_two, ffn_up, preferred_element_type=jnp.float32),
        ],
        axis=1,
    )
    hidden_units = ffn_gate.shape[1]
    summed = owned_sums(partial_two, squares_two)
    hidden = (jax.nn.silu(summed[:, :hidden_units]) * summed[:, hidden_units:]).astype(jnp.bfloat16)
    down_part = jnp.dot(
        gather_directly(hidden, "kv", 0), ffn_down, preferred_element_type=jnp.float32
    )
    down_sums = sent_and_summed(down_part.astype(jnp.bfloat16), "tp", 1)
    layer_output = (residual.astype(jnp.float32) + down_sums).astype(jnp.bfloat16)
    return (layer_output, new_state)


def solution(mesh):
    in_specs = (
        P(None, ("kv", "tp")),
        P("kv"),
        P("kv", "tp", None, None),
        P("kv"),
        P("kv", "tp"),
        P("kv", "tp"),
        P("kv", "tp"),
        P("kv", "tp"),
        P("tp", "kv"),
        P("kv"),
        P("kv", "tp"),
        P("kv", "tp"),
        P("tp", "kv"),
    )
    out_specs = (P(None, ("kv", "tp")), P("kv", "tp", None, None))
    return jax.shard_map(
        on_device, mesh=mesh, in_specs=in_specs, out_specs=out_specs, check_vma=False
    )
```

profile of v0, /device:TPU:1, one launch (start us, length us, event | category | flops | bytes accessed | tf_op | source)
XLA Modules:
  0.0 126.4 jit_solution(4354620266394448964)
XLA Ops:
  0.6 0.0 copy-start
  0.6 0.0 copy-start.2
  0.7 21.8 %all_gather.6 = bf16[128,256]{0,1:T(8,128)(2,1)S(1)} all-gather(bf16[128,16]{0,1:T(8,128)(2,1)} %param.13), channel_id=1, replica_groups=mesh['kv'=16,'tp'=16] {'tp'}, dimensions={1}, use_global_device_ids=true | all-gather | bytes 69632 | tf_op jit(solution)/shard_map/all_gather | solution.py:67
  22.5 0.1 fusion.12
  22.6 0.2 convert_element_type.141
  22.8 1.8 %fusion.5 = bf16[16,8,769]{2,1,0:T(8,128)(2,1)} fusion(bf16[256,128]{1,0:T(8,128)(2,1)} %param.17, bf16[128,256]{0,1:T(8,128)(2,1)S(1)} %all_gather.6, f32[256]{0:T(256)} %param.16), kind=kOutput, calls=%fused_computation.13 | convolution fusion | flops 8503295 | bytes 164864 | tf_op jit(solution)/shard_map/dot_general | solution.py:98
  24.6 1.8 %fusion.7 = bf16[16,8,769]{2,1,0:T(8,128)(2,1)} fusion(bf16[16,8,769]{2,1,0:T(8,128)(2,1)} %fusion.5, bf16[256,128]{1,0:T(8,128)(2,1)} %param.18, bf16[128,256]{0,1:T(8,128)(2,1)S(1)} %all_gather.6, f32[256]{0:T(256)} %param.16), kind=kOutput, calls=%fused_computation.15 | convolution fusion | flops 8503296 | bytes 164864 | tf_op jit(solution)/shard_map/dot_general | solution.py:99
  26.3 1.8 %fusion.1 = bf16[16,8,769]{2,1,0:T(8,128)(2,1)} fusion(bf16[16,8,769]{2,1,0:T(8,128)(2,1)} %fusion.7, bf16[256,256]{1,0:T(8,128)(2,1)} %param.19, bf16[128,256]{0,1:T(8,128)(2,1)S(1)} %all_gather.6, f32[256]{0:T(256)} %param.16), kind=kOutput, calls=%fused_computation.7 | convolution fusion | flops 16908288 | bytes 263168 | tf_op jit(solution)/shard_map/dot_general | solution.py:100
  28.1 1.8 %fusion.3 = bf16[16,8,769]{2,1,0:T(8,128)(2,1)} fusion(bf16[16,8,769]{2,1,0:T(8,128)(2,1)} %fusion.1, bf16[256,256]{1,0:T(8,128)(2,1)} %param.20, bf16[128,256]{0,1:T(8,128)(2,1)S(1)} %all_gather.6, f32[256]{0:T(256)} %param.16), kind=kOutput, calls=%fused_computation.9 | convolution fusion | flops 16908288 | bytes 263168 | tf_op jit(solution)/shard_map/dot_general | solution.py:101
  30.0 0.6 constant_dynamic-update-slice_fusion
  30.6 6.8 %all-to-all-start = ((bf16[16,8,769]{2,1,0:T(8,128)(2,1)}), bf16[16,8,769]{2,1,0:T(8,128)(2,1)S(1)}, u32[]{:S(2)}, u32[]{:S(2)}) async-start(bf16[16,8,769]{2,1,0:T(8,128)(2,1)} %constant_dynamic-update-slice_fusion), calls=%async_computation | async-start | bytes 458752 | tf_op jit(solution)/shard_map/all_to_all | solution.py:19
  37.4 0.0 copy-start.8
  37.4 0.6 copy-done.8
  38.1 7.3 %all-to-all-done = bf16[16,8,769]{2,1,0:T(8,128)(2,1)S(1)} async-done(((bf16[16,8,769]{2,1,0:T(8,128)(2,1)}), bf16[16,8,769]{2,1,0:T(8,128)(2,1)S(1)}, u32[]{:S(2)}, u32[]{:S(2)}) %all-to-all-start) | async-done | bytes 196896 | tf_op jit(solution)/shard_map/all_to_all | solution.py:19
  45.4 0.1 fusion.44
  45.5 0.1 slice_multiply_fusion.2
  45.6 0.1 fusion.49
  45.7 0.1 maximum_bitcast_fusion
  45.8 0.1 fusion.47
  45.9 0.0 copy-done.2
  45.9 0.2 multiply_add_fusion
  46.1 0.0 copy-start.1
  46.1 0.5 fusion.8
  46.6 0.0 copy-start.5
  46.6 0.1 fusion.19
  46.7 0.1 fusion.21
  46.8 9.2 %all_to_all.30 = bf16[16,8,256]{2,1,0:T(8,128)(2,1)S(1)} all-to-all(bf16[16,8,256]{2,1,0:T(8,128)(2,1)S(1)} %broadcast_in_dim.4), channel_id=1, replica_groups=mesh['kv'=16,'tp'=16] {'kv'}, dimensions={0} | all-to-all | bytes 131072 | tf_op jit(solution)/shard_map/all_to_all | solution.py:36
  55.9 0.0 copy-done.5
  56.0 0.2 convolution_convert_fusion.3
  56.1 0.1 copy.37
  56.2 13.9 %all_to_all.31 = bf16[16,128,16]{1,2,0:T(8,128)(2,1)S(1)} all-to-all(bf16[16,128,16]{1,2,0:T(8,128)(2,1)S(1)} %bitcast.66), channel_id=1, replica_groups=mesh['kv'=16,'tp'=16] {'tp'}, dimensions={0} | all-to-all | bytes 131072 | tf_op jit(solution)/shard_map/all_to_all | solution.py:19
  70.2 0.0 copy-start.6
  70.2 0.7 copy-done.6
  70.9 14.9 %all_gather.7 = bf16[128,256]{0,1:T(8,128)(2,1)S(1)} all-gather(bf16[128,16]{0,1:T(8,128)(2,1)S(1)} %add_convert_fusion.1), channel_id=1, replica_groups=mesh['kv'=16,'tp'=16] {'tp'}, dimensions={1}, use_global_device_ids=true | all-gather | bytes 69632 | tf_op jit(solution)/shard_map/all_gather | solution.py:67
  85.7 0.1 fusion.14
  85.8 0.0 copy-start.7
  85.8 0.2 convert_element_type.142
  86.0 0.0 copy-done
  86.0 0.4 copy-done.7
  86.5 0.0 copy-start.3
  86.5 0.3 convolution_convert_fusion.1
  86.8 0.0 copy-done.1
  86.8 0.1 copy.38
  86.9 0.5 copy-done.3
  87.4 0.3 convolution_convert_fusion
  87.8 0.1 copy.39
  87.9 0.2 concatenate.65
  88.1 12.3 %all_to_all.32 = bf16[16,8,1409]{2,1,0:T(8,128)(2,1)S(1)} all-to-all(bf16[16,8,1409]{2,1,0:T(8,128)(2,1)S(1)} %concatenate.65), channel_id=1, replica_groups=mesh['kv'=16,'tp'=16] {'kv'}, dimensions={0} | all-to-all | bytes 721408 | tf_op jit(solution)/shard_map/all_to_all | solution.py:19
  100.4 0.1 convert_reduce_fusion
  100.5 0.1 fusion.41
  100.6 0.0 copy-start.4
  100.6 0.1 slice_multiply_fusion
  100.7 0.1 fusion.18
  100.8 10.4 %all_to_all.33 = bf16[16,8,704]{2,1,0:T(8,128)(2,1)S(1)} all-to-all(bf16[16,8,704]{2,1,0:T(8,128)(2,1)S(1)} %broadcast_in_dim.5), channel_id=1, replica_groups=mesh['kv'=16,'tp'=16] {'kv'}, dimensions={0} | all-to-all | bytes 360448 | tf_op jit(solution)/shard_map/all_to_all | solution.py:36
  111.1 0.0 copy-done.4
  111.1 0.2 convolution_convert_fusion.2
  111.4 0.1 copy.41
  111.5 14.3 %all_to_all.34 = bf16[16,128,16]{1,2,0:T(8,128)(2,1)S(1)} all-to-all(bf16[16,128,16]{1,2,0:T(8,128)(2,1)S(1)} %bitcast.67), channel_id=1, replica_groups=mesh['kv'=16,'tp'=16] {'tp'}, dimensions={0} | all-to-all | bytes 131072 | tf_op jit(solution)/shard_map/all_to_all | solution.py:19
  125.8 0.6 add_convert_fusion
  (11 shorter events, 0.1 us)
Async XLA Ops:
  0.6 85.4 %copy-start = (bf16[256,704]{0,1:T(8,128)(2,1)S(1)}, bf16[256,704]{0,1:T(8,128)(2,1)}, u32[]{:S(2)}) copy-start(bf16[256,704]{0,1:T(8,128)(2,1)} %param.23) | copy-start | bytes 1081348
  0.6 45.2 %copy-start.2 = (f32[8,1,128,256]{3,2,1,0:T(8,128)S(1)}, f32[8,1,128,256]{3,2,1,0:T(8,128)}, u32[]{:S(2)}) copy-start(f32[8,1,128,256]{3,2,1,0:T(8,128)} %param.15) | copy-start | bytes 3145732
  30.6 14.7 %all-to-all-start = ((bf16[16,8,769]{2,1,0:T(8,128)(2,1)}), bf16[16,8,769]{2,1,0:T(8,128)(2,1)S(1)}, u32[]{:S(2)}, u32[]{:S(2)}) async-start(bf16[16,8,769]{2,1,0:T(8,128)(2,1)} %constant_dynamic-update-slice_fusion), calls=%async_computation | async-start | bytes 458752 | tf_op jit(solution)/shard_map/all_to_all | solution.py:19
  37.4 0.7 copy-start.8
  46.1 40.7 %copy-start.1 = (f32[8,1,128,256]{3,2,1,0:T(8,128)}, f32[8,1,128,256]{3,2,1,0:T(8,128)S(1)}, u32[]{:S(2)}) copy-start(f32[8,1,128,256]{3,2,1,0:T(8,128)S(1)} %multiply_add_fusion) | copy-start | bytes 3145732
  46.6 9.4 %copy-start.5 = (bf16[256,256]{1,0:T(8,128)(2,1)S(1)}, bf16[256,256]{1,0:T(8,128)(2,1)}, u32[]{:S(2)}) copy-start(bf16[256,256]{1,0:T(8,128)(2,1)} %param.21) | copy-start | bytes 393220
  70.2 0.7 copy-start.6
  85.8 0.7 copy-start.7
  86.5 1.0 copy-start.3
  100.6 10.6 %copy-start.4 = (bf16[704,256]{1,0:T(8,128)(2,1)S(1)}, bf16[704,256]{1,0:T(8,128)(2,1)}, u32[]{:S(2)}) copy-start(bf16[704,256]{1,0:T(8,128)(2,1)} %param.25) | copy-start | bytes 1081348
where the time goes:
time: 127 us; the launch traced here: 126 us
  blocking collectives  96.8 us (76%)
  matrix products  8.66 us (7%)
  waiting for transfers between devices  7.25 us (6%)
  starting transfers between devices  6.75 us (5%)
  local copies, waits for them, and re-layouts  4.08 us (3%)
  other arithmetic  1.99 us (2%)
    all_to_all x3, blocking collectives, sent_and_summed(): lax.all_to_all(blocks, axis, split_axis=0, concat_axis=0, tiled=True)  40.5 us
    all_gather x2, blocking collectives, gathered_rows(): return lax.all_gather(columns, 'tp', axis=1, tiled=True)  36.7 us
    all_to_all x2, blocking collectives, copy_for_each(): lax.all_to_all(jnp.broadcast_to(value[None], (devices, *value.shape)), ax...  19.6 us
    all_to_all x1, waiting for transfers between devices, sent_and_summed(): lax.all_to_all(blocks, axis, split_axis=0, concat_axis=0, tiled=True)  7.25 us
    all_to_all x1, starting transfers between devices, sent_and_summed(): lax.all_to_all(blocks, axis, split_axis=0, concat_axis=0, tiled=True)  6.75 us
  transfers between devices with their start and end apart: 1, of which 1 were waited for; matrix products, arithmetic and copies ran while one was open for 0% of the time, Pallas kernels for 0%

commit v1 on v0

--- a/solution.py
+++ b/solution.py
@@ -1,3 +1,4 @@
+import functools
 import jax
 import jax.numpy as jnp
 from jax import lax
@@ -6,6 +7,19 @@
 D = 4096
 HEADS = 16
 QK = 128
+
+
+def _fix_levels_all(point, out_dim):
+    return lax.all_to_all(
+        jnp.concatenate([point] * lax.axis_size("tp"), axis=out_dim),
+        "tp",
+        out_dim,
+        out_dim,
+        tiled=True,
+    )
+
+
+record_state = functools.partial(_fix_levels_all, out_dim=1)
 
 
 def in_blocks(value, dim, devices):
@@ -64,7 +78,7 @@
 
 
 def gathered_rows(columns):
-    return lax.all_gather(columns, "tp", axis=1, tiled=True)
+    return record_state(columns)
 
 
 def owned_sums(partial_value, squares):

time: 127 us -> 114 us (0.90)
  blocking collectives: 96.8 us -> 85.4 us
  matrix products: 8.66 us -> 4.5 us
  local copies, waits for them, and re-layouts: 4.08 us -> 6.3 us
    all_gather x2 -> x0, blocking collectives: 36.7 us -> none  [gathered_rows(): return lax.all_gather(columns, 'tp', axis=1, tiled=True)]
    all_to_all x0 -> x2, blocking collectives: none -> 27.9 us  [_fix_levels_all(): lax.all_to_all(jnp.concatenate([point] * lax.axis_size('tp'), axis=out_di...]
    all_to_all x3, blocking collectives: 40.5 us -> 37.9 us  [sent_and_summed(): lax.all_to_all(blocks, axis, split_axis=0, concat_axis=0, tiled=True)]
    convert_element_type x0 -> x4, local copies, waits for them, and re-layouts: none -> 1.78 us  [the longest x2 0.89 us: on_device(): feature_block = gathered_rows(tokens).astype(jnp.float32)]
    unnamed x18 -> x57, local copies, waits for them, and re-layouts: 2.27 us -> 2.99 us
where the time goes in v1:
time: 114 us; the launch traced here: 113 us
  blocking collectives  85.4 us (75%)
  waiting for transfers between devices  7.3 us (6%)
  starting transfers between devices  6.76 us (6%)
  local copies, waits for them, and re-layouts  6.3 us (6%)
  matrix products  4.5 us (4%)
  other arithmetic  2 us (2%)
    all_to_all x3, blocking collectives, sent_and_summed(): lax.all_to_all(blocks, axis, split_axis=0, concat_axis=0, tiled=True)  37.9 us
    all_to_all x2, blocking collectives, _fix_levels_all(): lax.all_to_all(jnp.concatenate([point] * lax.axis_size('tp'), axis=out_di...  27.9 us
    all_to_all x2, blocking collectives, copy_for_each(): lax.all_to_all(jnp.broadcast_to(value[None], (devices, *value.shape)), ax...  19.6 us
    all_to_all x1, waiting for transfers between devices, sent_and_summed(): lax.all_to_all(blocks, axis, split_axis=0, concat_axis=0, tiled=True)  7.3 us
    all_to_all x1, starting transfers between devices, sent_and_summed(): lax.all_to_all(blocks, axis, split_axis=0, concat_axis=0, tiled=True)  6.76 us
    unnamed x57, local copies, waits for them, and re-layouts  2.99 us
  transfers between devices with their start and end apart: 1, of which 1 were waited for; matrix products, arithmetic and copies ran while one was open for 0% of the time, Pallas kernels for 0%

profile of v1, /device:TPU:1, one launch (start us, length us, event | category | flops | bytes accessed | tf_op | source)
XLA Modules:
  0.0 113.3 jit_solution(14538176227332757618)
XLA Ops:
  0.6 0.0 copy-start
  0.6 0.0 copy-start.2
  0.7 0.8 constant_dynamic-update-slice_fusion.15
  1.4 0.0 copy-done.2
  1.6 17.5 %all_to_all.48 = bf16[128,16,16]{0,2,1:T(8,128)(2,1)S(1)} all-to-all(bf16[128,16,16]{0,2,1:T(8,128)(2,1)S(1)} %bitcast.67), channel_id=1, replica_groups=mesh['kv'=16,'tp'=16] {'tp'}, dimensions={1} | all-to-all | bytes 131072 | tf_op jit(solution)/shard_map/all_to_all | solution.py:13
  19.1 0.1 multiply_reduce_fusion.1
  19.2 0.2 convert_element_type.171
  19.4 0.5 copy.39
  19.9 0.0 copy-start.12
  19.9 0.0 copy-start.9
  19.9 0.0 copy-start.10
  19.9 0.0 copy-start.6
  19.9 0.0 copy-start.7
  19.9 0.4 reshape.296
  20.4 0.2 copy-done.12
  20.6 0.2 copy-done.9
  20.7 0.8 fusion.3
  21.5 0.0 copy-done.10
  21.5 0.8 fusion.2
  22.3 0.0 copy-done.6
  22.3 0.8 fusion.1
  23.1 0.0 copy-done.7
  23.1 0.8 fusion
  23.9 0.6 constant_dynamic-update-slice_fusion.16
  24.5 6.8 %all-to-all-start.1 = ((bf16[16,8,769]{2,1,0:T(8,128)(2,1)}), bf16[16,8,769]{2,1,0:T(8,128)(2,1)S(1)}, u32[]{:S(2)}, u32[]{:S(2)}) async-start(bf16[16,8,769]{2,1,0:T(8,128)(2,1)} %constant_dynamic-update-slice_fusion.16), calls=%async_computation.1 | async-start | bytes 458752 | tf_op jit(solution)/shard_map/all_to_all | solution.py:33
  31.3 0.0 copy-start.13
  31.3 0.6 copy-done.13
  32.0 7.3 %all-to-all-done.1 = bf16[16,8,769]{2,1,0:T(8,128)(2,1)S(1)} async-done(((bf16[16,8,769]{2,1,0:T(8,128)(2,1)}), bf16[16,8,769]{2,1,0:T(8,128)(2,1)S(1)}, u32[]{:S(2)}, u32[]{:S(2)}) %all-to-all-start.1) | async-done | bytes 196896 | tf_op jit(solution)/shard_map/all_to_all | solution.py:33
  39.3 0.1 fusion.40
  39.4 0.1 slice_multiply_fusion.2
  39.5 0.1 fusion.45
  39.7 0.1 maximum_bitcast_fusion
  39.7 0.1 fusion.43
  39.8 0.2 multiply_add_fusion
  40.0 0.0 copy-start.1
  40.0 0.5 fusion.4
  40.5 0.1 fusion.15
  40.6 0.1 fusion.17
  40.7 9.2 %all_to_all.49 = bf16[16,8,256]{2,1,0:T(8,128)(2,1)S(1)} all-to-all(bf16[16,8,256]{2,1,0:T(8,128)(2,1)S(1)} %broadcast_in_dim.4), channel_id=1, replica_groups=mesh['kv'=16,'tp'=16] {'kv'}, dimensions={0} | all-to-all | bytes 131072 | tf_op jit(solution)/shard_map/all_to_all | solution.py:50
  49.9 0.2 convolution_convert_fusion.3
  50.1 0.1 copy.41
  50.2 12.9 %all_to_all.50 = bf16[16,128,16]{1,2,0:T(8,128)(2,1)S(1)} all-to-all(bf16[16,128,16]{1,2,0:T(8,128)(2,1)S(1)} %bitcast.64), channel_id=1, replica_groups=mesh['kv'=16,'tp'=16] {'tp'}, dimensions={0} | all-to-all | bytes 131072 | tf_op jit(solution)/shard_map/all_to_all | solution.py:33
  63.3 10.4 %all_to_all.51 = bf16[128,16,16]{0,2,1:T(8,128)(2,1)S(1)} all-to-all(bf16[128,16,16]{0,2,1:T(8,128)(2,1)S(1)} %bitcast.66), channel_id=1, replica_groups=mesh['kv'=16,'tp'=16] {'tp'}, dimensions={1} | all-to-all | bytes 131072 | tf_op jit(solution)/shard_map/all_to_all | solution.py:13
  73.7 0.1 multiply_reduce_fusion
  73.7 0.2 convert_element_type.172
  74.0 0.5 copy.42
  74.4 0.0 copy-start.11
  74.4 0.4 reshape.299
  74.9 0.2 copy-done.11
  75.1 0.3 convolution_convert_fusion
  75.4 0.7 copy-done.5
  76.1 0.3 convolution_convert_fusion.1
  76.4 0.2 concatenate.55
  76.6 12.3 %all_to_all.52 = bf16[16,8,1409]{2,1,0:T(8,128)(2,1)S(1)} all-to-all(bf16[16,8,1409]{2,1,0:T(8,128)(2,1)S(1)} %concatenate.55), channel_id=1, replica_groups=mesh['kv'=16,'tp'=16] {'kv'}, dimensions={0} | all-to-all | bytes 721408 | tf_op jit(solution)/shard_map/all_to_all | solution.py:33
  88.9 0.1 convert_reduce_fusion
  88.9 0.1 fusion.37
  89.1 0.1 slice_multiply_fusion
  89.1 0.1 fusion.14
  89.2 10.4 %all_to_all.53 = bf16[16,8,704]{2,1,0:T(8,128)(2,1)S(1)} all-to-all(bf16[16,8,704]{2,1,0:T(8,128)(2,1)S(1)} %broadcast_in_dim.5), channel_id=1, replica_groups=mesh['kv'=16,'tp'=16] {'kv'}, dimensions={0} | all-to-all | bytes 360448 | tf_op jit(solution)/shard_map/all_to_all | solution.py:50
  99.6 0.0 copy-done.4
  99.6 0.2 convolution_convert_fusion.2
  99.8 0.1 copy.44
  99.9 12.7 %all_to_all.54 = bf16[16,128,16]{1,2,0:T(8,128)(2,1)S(1)} all-to-all(bf16[16,128,16]{1,2,0:T(8,128)(2,1)S(1)} %bitcast.65), channel_id=1, replica_groups=mesh['kv'=16,'tp'=16] {'tp'}, dimensions={0} | all-to-all | bytes 131072 | tf_op jit(solution)/shard_map/all_to_all | solution.py:33
  112.7 0.6 add_convert_fusion
  (50 shorter events, 0.4 us)
Async XLA Ops:
  0.6 74.3 %copy-start = (bf16[256,704]{0,1:T(8,128)(2,1)S(1)}, bf16[256,704]{0,1:T(8,128)(2,1)}, u32[]{:S(2)}) copy-start(bf16[256,704]{0,1:T(8,128)(2,1)} %param.24) | copy-start | bytes 1081348
  0.6 0.8 copy-start.2
  19.9 0.7 copy-start.12
  19.9 0.8 copy-start.9
  19.9 1.6 %copy-start.10 = (bf16[256,128]{1,0:T(8,128)(2,1)S(1)}, bf16[256,128]{1,0:T(8,128)(2,1)}, u32[]{:S(2)}) copy-start(bf16[256,128]{1,0:T(8,128)(2,1)} %param.18) | copy-start | bytes 196612
  19.9 2.4 %copy-start.6 = (bf16[256,256]{1,0:T(8,128)(2,1)S(1)}, bf16[256,256]{1,0:T(8,128)(2,1)}, u32[]{:S(2)}) copy-start(bf16[256,256]{1,0:T(8,128)(2,1)} %param.19) | copy-start | bytes 393220
  19.9 3.2 %copy-start.7 = (bf16[256,256]{1,0:T(8,128)(2,1)S(1)}, bf16[256,256]{1,0:T(8,128)(2,1)}, u32[]{:S(2)}) copy-start(bf16[256,256]{1,0:T(8,128)(2,1)} %param.20) | copy-start | bytes 393220
  20.5 19.3 %copy-start.3 = (f32[8,1,128,256]{3,2,1,0:T(8,128)S(1)}, f32[8,1,128,256]{3,2,1,0:T(8,128)}, u32[]{:S(2)}) copy-start(f32[8,1,128,256]{3,2,1,0:T(8,128)} %param.15) | copy-start | bytes 3145732
  24.5 14.8 %all-to-all-start.1 = ((bf16[16,8,769]{2,1,0:T(8,128)(2,1)}), bf16[16,8,769]{2,1,0:T(8,128)(2,1)S(1)}, u32[]{:S(2)}, u32[]{:S(2)}) async-start(bf16[16,8,769]{2,1,0:T(8,128)(2,1)} %constant_dynamic-update-slice_fusion.16), calls=%async_computation.1 | async-start | bytes 458752 | tf_op jit(solution)/shard_map/all_to_all | solution.py:33
  31.3 0.7 copy-start.13
  40.0 33.7 %copy-start.1 = (f32[8,1,128,256]{3,2,1,0:T(8,128)}, f32[8,1,128,256]{3,2,1,0:T(8,128)S(1)}, u32[]{:S(2)}) copy-start(f32[8,1,128,256]{3,2,1,0:T(8,128)S(1)} %multiply_add_fusion) | copy-start | bytes 3145732
  40.5 9.4 %copy-start.8 = (bf16[256,256]{1,0:T(8,128)(2,1)S(1)}, bf16[256,256]{1,0:T(8,128)(2,1)}, u32[]{:S(2)}) copy-start(bf16[256,256]{1,0:T(8,128)(2,1)} %param.21) | copy-start | bytes 393220
  74.4 0.7 copy-start.11
  75.1 1.0 copy-start.5
  89.0 10.6 %copy-start.4 = (bf16[704,256]{1,0:T(8,128)(2,1)S(1)}, bf16[704,256]{1,0:T(8,128)(2,1)}, u32[]{:S(2)}) copy-start(bf16[704,256]{1,0:T(8,128)(2,1)} %param.25) | copy-start | bytes 1081348
